TPU v7x, 128 devices: a whole 4x4x4 slice. The times are simulated.
128 devices in a mesh: fs: 16 (over z, y), tp: 8 (over x, core).
Axes of the slice: x: 4, y: 4, z: 4, core: 2. Of those that a mesh axis runs over, the one named last changes fastest.
Arguments:
- tokens: bfloat16 [8192, 4096], P('fs'), may hold values from -6 to 6
- norm_gain: float32 [4096], P('fs'), may hold values from 0.1 to 1.9
- gate_train: float32 [16, 4096, 1024], P(None, 'fs', 'tp'), may hold values from -0.09375 to 0.09375
- up_train: float32 [16, 4096, 1024], P(None, 'fs', 'tp'), may hold values from -0.09375 to 0.09375
- down_train: float32 [16, 1024, 4096], P(None, 'fs', 'tp'), may hold values from -0.1875 to 0.1875
- shared_gate_train: float32 [4096, 1024], P('fs', 'tp'), may hold values from -0.09375 to 0.09375
- shared_up_train: float32 [4096, 1024], P('fs', 'tp'), may hold values from -0.09375 to 0.09375
- shared_down_train: float32 [1024, 4096], P('fs', 'tp'), may hold values from -0.1875 to 0.1875
- route_expert: int32 [8192, 2], P('fs'), may hold values from 0 to 15, all different within a row; in each aligned block of 512 rows (0 to 511, 512 to 1023, ...) at most 96 rows name the same one
- route_weight: float32 [8192, 2], P('fs'), may hold values from 0.1 to 1
Outputs:
- expert_gate: bfloat16 [16, 4096, 1024], P('fs', None, 'tp')
- expert_up: bfloat16 [16, 4096, 1024], P('fs', None, 'tp')
- expert_down: bfloat16 [16, 1024, 4096], P('fs', 'tp')
- shared_gate: bfloat16 [4096, 1024], P(None, 'tp')
- shared_up: bfloat16 [4096, 1024], P(None, 'tp')
- shared_down: bfloat16 [1024, 4096], P('tp')
- mixed: bfloat16 [8192, 4096], P('fs', 'tp')
Inputs may be any that keep to these rules, and one draw needn't show every extreme that they name: `route_expert`: each row names 2 different experts. Within each aligned block of 512 rows no expert is named by more than 96 rows, a bound that some block reaches in every draw.
All inputs are finite; a program needn't handle non-finite values.
Results may differ from a plain program's by a relative error of at most 0.015.
Values may be sent and summed in bfloat16 or wider, within the bound.
No kernel may reach another device: no remote copies, remote signals or barrier semaphores. Data moves between devices by JAX's collectives and lax.ppermute only.
A program may use at most 128 MiB of HBM per device.

v0:
```python
import jax
import jax.numpy as jnp
from jax import lax
from jax.sharding import PartitionSpec as P

norm_eps = 1e-06


def sent_together(arrays, axis, dim, along):
    widths = [a.shape[along] for a in arrays]
    both = jnp.concatenate(arrays, axis=along)
    result = lax.all_gather(both, axis, axis=dim, tiled=True)
    return tuple(jnp.split(result, [sum(widths[:k]) for k in range(1, len(widths))], axis=along))


def blockwise_down(hidden, weight_down, pieces):
    step_width = hidden.shape[1] // pieces
    total = jnp.zeros((hidden.shape[0], weight_down.shape[1]), jnp.float32)
    for block in range(pieces):
        term = jnp.dot(
            hidden[:, block * step_width : (block + 1) * step_width],
            weight_down[block * step_width : (block + 1) * step_width],
            preferred_element_type=jnp.float32,
        )
        total = total + term.astype(jnp.bfloat16).astype(jnp.float32)
    return total


def on_device(
    tokens,
    norm_gain,
    gate_train,
    up_train,
    down_train,
    shared_gate_train,
    shared_up_train,
    shared_down_train,
    route_expert,
    route_weight,
):
    gain_rows = norm_gain[None, :, None]
    gate_local = (gain_rows * gate_train).astype(jnp.bfloat16)
    up_local = (gain_rows * up_train).astype(jnp.bfloat16)
    expert_gate, expert_up = (
        lax.all_to_all(gate_local, "fs", split_axis=0, concat_axis=1, tiled=True),
        lax.all_to_all(up_local, "fs", split_axis=0, concat_axis=1, tiled=True),
    )
    expert_down = lax.all_to_all(
        lax.all_to_all(
            down_train.astype(jnp.bfloat16), "fs", split_axis=0, concat_axis=1, tiled=True
        ),
        "tp",
        split_axis=1,
        concat_axis=2,
        tiled=True,
    )
    shared_gate_local = (norm_gain[:, None] * shared_gate_train).astype(jnp.bfloat16)
    shared_up_local = (norm_gain[:, None] * shared_up_train).astype(jnp.bfloat16)
    shared_gate, shared_up, shared_down_rows = (
        *sent_together((shared_gate_local, shared_up_local), "fs", 0, 1),
        lax.all_gather(shared_down_train.astype(jnp.bfloat16), "fs", axis=0, tiled=True),
    )
    shared_down = lax.all_to_all(shared_down_rows, "tp", split_axis=0, concat_axis=1, tiled=True)
    tok_rows, model_width = tokens.shape
    top_count = route_expert.shape[1]
    experts = lax.axis_size("fs")
    pieces = lax.axis_size("tp")
    capacity = 3 * tok_rows * top_count // (2 * experts)
    columns = model_width // pieces
    values = tokens.astype(jnp.float32)
    normed = (
        values * lax.rsqrt(jnp.mean(values * values, axis=1, keepdims=True) + norm_eps)
    ).astype(jnp.bfloat16)
    pairs = route_expert.reshape(-1)
    chosen = (pairs[:, None] == jnp.arange(experts, dtype=jnp.int32)[None, :]).astype(jnp.int32)
    earlier = jnp.cumsum(chosen, axis=0) - chosen
    slot_of = jnp.sum(earlier * chosen, axis=1)
    target = pairs * capacity + slot_of
    matches = (target[:, None] == jnp.arange(experts * capacity, dtype=jnp.int32)[None, :]).astype(
        jnp.bfloat16
    )
    placing = jnp.sum(matches.reshape(tok_rows, top_count, experts * capacity), axis=1)
    own_columns = lax.dynamic_slice_in_dim(normed, lax.axis_index("tp") * columns, columns, 1)
    outgoing = jnp.einsum("ts,td->sd", placing, own_columns, preferred_element_type=jnp.float32)
    outgoing = outgoing.astype(jnp.bfloat16).reshape(experts, capacity, columns)
    arriving = lax.all_to_all(outgoing, "fs", split_axis=0, concat_axis=0, tiled=True)
    arrived = lax.all_gather(arriving, "tp", axis=2, tiled=True)
    arrived_rows = arrived.reshape(-1, model_width)
    gate_vals = jnp.dot(arrived_rows, expert_gate[0], preferred_element_type=jnp.float32)
    up_vals = jnp.dot(arrived_rows, expert_up[0], preferred_element_type=jnp.float32)
    expert_hidden = (jax.nn.silu(gate_vals) * up_vals).astype(jnp.bfloat16)
    shared_gate_vals = jnp.dot(normed, shared_gate, preferred_element_type=jnp.float32)
    shared_up_vals = jnp.dot(normed, shared_up, preferred_element_type=jnp.float32)
    shared_hidden = (jax.nn.silu(shared_gate_vals) * shared_up_vals).astype(jnp.bfloat16)
    down_by_columns = lax.all_to_all(expert_down[0], "tp", split_axis=1, concat_axis=0, tiled=True)
    hidden_whole, shared_whole = sent_together((expert_hidden, shared_hidden), "tp", 1, 0)
    expert_sums = blockwise_down(hidden_whole, down_by_columns, pieces)
    shared_sums = blockwise_down(shared_whole, shared_down_rows, pieces)
    returning = expert_sums.astype(jnp.bfloat16).reshape(experts, capacity, columns)
    returned = lax.all_to_all(returning, "fs", split_axis=0, concat_axis=0, tiled=True).reshape(
        experts * capacity, columns
    )
    picked = jnp.take(returned, target, axis=0).reshape(tok_rows, top_count, columns)
    routed = jnp.sum(route_weight[:, :, None] * picked.astype(jnp.float32), axis=1)
    mixed = (routed + shared_sums).astype(jnp.bfloat16)
    return (expert_gate, expert_up, expert_down, shared_gate, shared_up, shared_down, mixed)


def solution(mesh):
    placed = (
        P("fs", None),
        P("fs"),
        P(None, "fs", "tp"),
        P(None, "fs", "tp"),
        P(None, "fs", "tp"),
        P("fs", "tp"),
        P("fs", "tp"),
        P("fs", "tp"),
        P("fs", None),
        P("fs", None),
    )
    return jax.shard_map(
        on_device,
        mesh=mesh,
        in_specs=placed,
        out_specs=(
            P("fs", None, "tp"),
            P("fs", None, "tp"),
            P("fs", "tp", None),
            P(None, "tp"),
            P(None, "tp"),
            P("tp", None),
            P("fs", "tp"),
        ),
        check_vma=False,
    )
```

profile of v0, /device:TPU:0, one launch (start us, length us, event | category | flops | bytes accessed | tf_op | source)
XLA Modules:
  0.0 312.0 jit_solution(5884856145658552887)
XLA Ops:
  10.2 4.5 %reduce-window.6 = s32[16,8,128]{2,1,0:T(8,128)S(1)} reduce-window(s32[16,8,128]{2,1,0:T(8,128)S(1)} %fusion.51, s32[]{:T(128)} %constant.18.clone.1), window={size=1x1x128 pad=0_0x0_0x127_0}, to_apply=%region_0.0 | reduce-window | flops 2080768 | bytes 131076 | tf_op jit(solution)/shard_map/reduce-window
  17.0 3.1 fusion
  23.6 33.0 %all_to_all.99 = bf16[16,96,512]{2,1,0:T(8,128)(2,1)} all-to-all(bf16[16,96,512]{2,1,0:T(8,128)(2,1)S(1)} %bitcast.97), channel_id=1, replica_groups=mesh['fs'=16,'tp'=8] {'fs'}, dimensions={0} | all-to-all | bytes 3145728 | tf_op jit(solution)/shard_map/all_to_all | solution.py:86
  56.6 3.5 %multiply_convert_fusion = (bf16[16,256,128]{2,1,0:T(8,128)(2,1)}, bf16[16,256,128]{2,1,0:T(8,128)(2,1)}) fusion(f32[16,256,128]{2,1,0:T(8,128)S(1)} %copy-done.11, f32[256]{0:T(256)S(1)} %copy-done.16, f32[16,256,128]{2,1,0:T(8,128)} %param.12), kind=kLoop, calls=%fused_computation.21 | loop fusion | flops 2097152 | bytes 6292480 | tf_op jit(solution)/shard_map/convert_element_type | solution.py:43
  60.1 3.7 %all-to-all-start = ((bf16[16,256,128]{2,1,0:T(8,128)(2,1)}), bf16[16,256,128]{2,1,0:T(8,128)(2,1)S(1)}, u32[]{:S(2)}, u32[]{:S(2)}) async-start(bf16[16,256,128]{2,1,0:T(8,128)(2,1)} %get-tuple-element.49), calls=%async_computation | async-start | bytes 2097152 | tf_op jit(solution)/shard_map/all_to_all | solution.py:45
  64.6 1.8 fusion.55
  70.0 8.6 %all-to-all-done = bf16[16,256,128]{2,1,0:T(8,128)(2,1)S(1)} async-done(((bf16[16,256,128]{2,1,0:T(8,128)(2,1)}), bf16[16,256,128]{2,1,0:T(8,128)(2,1)S(1)}, u32[]{:S(2)}, u32[]{:S(2)}) %all-to-all-start) | async-done | bytes 1048608 | tf_op jit(solution)/shard_map/all_to_all | solution.py:45
  78.6 3.7 %all-to-all-start.1 = ((bf16[16,256,128]{2,1,0:T(8,128)(2,1)}), bf16[16,256,128]{2,1,0:T(8,128)(2,1)S(1)}, u32[]{:S(2)}, u32[]{:S(2)}) async-start(bf16[16,256,128]{2,1,0:T(8,128)(2,1)} %get-tuple-element.48), calls=%async_computation.1 | async-start | bytes 2097152 | tf_op jit(solution)/shard_map/all_to_all | solution.py:46
  82.3 51.0 %all-gather.9.cloned.1.call-done = bf16[16,96,4096]{2,1,0:T(8,128)(2,1)} async-done(((bf16[16,96,512]{2,1,0:T(8,128)(2,1)}), bf16[16,96,4096]{2,1,0:T(8,128)(2,1)}) %all-gather.9.cloned.1.call-update) | async-done | bytes 12582928 | tf_op jit(solution)/shard_map/all_gather | solution.py:87
  133.2 6.4 %fusion.56 = f32[1536,128]{1,0:T(8,128)S(1)} fusion(bf16[1536,4096]{1,0:T(8,128)(2,1)} %bitcast.102, bf16[4096,128]{1,0:T(8,128)(2,1)S(1)} %bitcast.91), kind=kOutput, calls=%fused_computation.106 | convolution fusion | flops 1610612736 | bytes 14417920 | tf_op jit(solution)/shard_map/dot_general | solution.py:89
  139.7 7.0 %fusion.4 = bf16[1536,128]{1,0:T(8,128)(2,1)S(1)} fusion(bf16[1536,4096]{1,0:T(8,128)(2,1)} %bitcast.103, bf16[4096,128]{1,0:T(8,128)(2,1)S(1)} %bitcast.93, f32[1536,128]{1,0:T(8,128)S(1)} %fusion.56), kind=kOutput, calls=%fused_computation.19 | convolution fusion | flops 1611792384 | bytes 14811136 | tf_op jit(solution)/shard_map/dot_general | solution.py:90
  147.6 1.7 convert_element_type.153
  149.3 25.8 %all_to_all.100 = bf16[16,64,512]{2,1,0:T(8,128)(2,1)S(1)} all-to-all(bf16[16,64,512]{2,1,0:T(8,128)(2,1)S(1)} %convert_element_type.153), channel_id=1, replica_groups=mesh['fs'=16,'tp'=8] {'fs'}, dimensions={0} | all-to-all | bytes 2097152 | tf_op jit(solution)/shard_map/all_to_all | solution.py:49
  175.1 1.6 copy.87
  177.2 7.0 %reduce.1 = bf16[1024,512]{1,0:T(8,128)(2,1)S(1)} reduce(bf16[1024,1,512]{2,1,0:T(2,128)(2,1)S(1)} %bitcast.80, bf16[]{:T(256)} %broadcast.91), dimensions={1}, to_apply=%bitcast.77.reduce_sub_computation | reduce | bytes 2097154
  185.0 24.0 %all_to_all.101 = bf16[8,2,32768]{2,1,0:T(2,128)(2,1)S(1)} all-to-all(bf16[8,2,32768]{2,1,0:T(2,128)(2,1)S(1)} %reshape.154), channel_id=1, replica_groups=mesh['fs'=16,'tp'=8] {'tp'}, dimensions={0} | all-to-all | bytes 2097152 | tf_op jit(solution)/shard_map/all_to_all | solution.py:48
  209.1 4.2 %all-to-all-start.4 = ((bf16[8,128,512]{2,1,0:T(8,128)(2,1)}), bf16[8,128,512]{2,1,0:T(8,128)(2,1)}, u32[]{:S(2)}, u32[]{:S(2)}) async-start(bf16[8,128,512]{2,1,0:T(8,128)(2,1)} %bitcast.89), calls=%async_computation.4 | async-start | bytes 2097152 | tf_op jit(solution)/shard_map/all_to_all | solution.py:63
  215.7 17.9 %all-to-all-done.4 = bf16[8,128,512]{2,1,0:T(8,128)(2,1)} async-done(((bf16[8,128,512]{2,1,0:T(8,128)(2,1)}), bf16[8,128,512]{2,1,0:T(8,128)(2,1)}, u32[]{:S(2)}, u32[]{:S(2)}) %all-to-all-start.4) | async-done | bytes 1048608 | tf_op jit(solution)/shard_map/all_to_all | solution.py:63
  233.6 3.8 %all-to-all-start.6 = ((bf16[128,8,512]{2,0,1:T(8,128)(2,1)}), bf16[128,8,512]{2,0,1:T(8,128)(2,1)S(1)}, u32[]{:S(2)}, u32[]{:S(2)}) async-start(bf16[128,8,512]{2,0,1:T(8,128)(2,1)} %bitcast.14), calls=%async_computation.6 | async-start | bytes 2097152 | tf_op jit(solution)/shard_map/all_to_all | solution.py:95
  238.1 1.6 copy.71
  241.0 1.6 copy.72
  244.0 9.3 %all-to-all-done.6 = bf16[128,8,512]{2,0,1:T(8,128)(2,1)S(1)} async-done(((bf16[128,8,512]{2,0,1:T(8,128)(2,1)}), bf16[128,8,512]{2,0,1:T(8,128)(2,1)S(1)}, u32[]{:S(2)}, u32[]{:S(2)}) %all-to-all-start.6) | async-done | bytes 1048608 | tf_op jit(solution)/shard_map/all_to_all | solution.py:95
  253.3 1.7 convolution_convert_fusion.7
  255.0 1.5 convolution_convert_fusion.6
  259.3 2.8 add_convert_fusion
  262.1 3.9 %all-to-all-start.7 = ((bf16[16,96,512]{2,1,0:T(8,128)(2,1)}), bf16[16,96,512]{2,1,0:T(8,128)(2,1)S(1)}, u32[]{:S(2)}, u32[]{:S(2)}) async-start(bf16[16,96,512]{2,1,0:T(8,128)(2,1)} %bitcast.24), calls=%async_computation.7 | async-start | bytes 3145728 | tf_op jit(solution)/shard_map/all_to_all | solution.py:100
  273.2 2.2 fusion.10
  275.4 15.1 %all-to-all-done.7 = bf16[16,96,512]{2,1,0:T(8,128)(2,1)S(1)} async-done(((bf16[16,96,512]{2,1,0:T(8,128)(2,1)}), bf16[16,96,512]{2,1,0:T(8,128)(2,1)S(1)}, u32[]{:S(2)}, u32[]{:S(2)}) %all-to-all-start.7) | async-done | bytes 1572896 | tf_op jit(solution)/shard_map/all_to_all | solution.py:100
  290.4 5.1 %gather_fusion = bf16[1024,512]{1,0:T(8,128)(2,1)} fusion(bf16[1536,512]{1,0:T(8,128)(2,1)S(1)} %bitcast.78, s32[1024]{0:T(1024)S(1)} %broadcast_clamp_fusion), kind=kCustom, calls=%fused_computation | custom fusion | bytes 2101248 | tf_op jit(solution)/shard_map/jit(_take)/gather | solution.py:103
  295.5 1.6 gather.7
  297.1 4.4 %multiply_reduce_fusion = f32[512,512]{1,0:T(8,128)S(1)} fusion(bf16[512,2,512]{2,1,0:T(2,128)(2,1)S(1)} %gather.7, pred[512,2]{1,0:T(8,128)(4,1)S(1)} %copy.79, f32[512,2]{1,0:T(8,128)S(1)} %copy.73), kind=kLoop, calls=%fused_computation.20 | loop fusion | flops 1835008 | bytes 2102272 | tf_op jit(solution)/shard_map/reduce_sum | solution.py:104
  301.5 2.0 fusion.8
  (96 shorter events, 32.6 us)
Async XLA Ops:
  7.2 57.4 %all-gather.5.cloned.1.call-start = ((), (), s32[]{:S(2)}) async-start(), calls=%async_computation.8 | async-start | bytes 2228224 | tf_op jit(solution)/shard_map/all_gather | solution.py:12
  9.0 124.2 %all-gather.9.cloned.1.call-start = ((), (), s32[]{:S(2)}) async-start(), calls=%async_computation.10 | async-start | bytes 14155776 | tf_op jit(solution)/shard_map/all_gather | solution.py:87
  15.5 4.6 %copy-start = (bf16[512,4096]{1,0:T(8,128)(2,1)S(1)}, bf16[512,4096]{1,0:T(8,128)(2,1)}, u32[]{:S(2)}) copy-start(bf16[512,4096]{1,0:T(8,128)(2,1)} %param.10) | copy-start | bytes 12582916
  21.6 1.9 copy-start.1
  23.6 33.0 %copy-start.11 = (f32[16,256,128]{2,1,0:T(8,128)S(1)}, f32[16,256,128]{2,1,0:T(8,128)}, u32[]{:S(2)}) copy-start(f32[16,256,128]{2,1,0:T(8,128)} %param.13) | copy-start | bytes 6291460
  23.6 33.0 %copy-start.16 = (f32[256]{0:T(256)S(1)}, f32[256]{0:T(256)}, u32[]{:S(2)}) copy-start(f32[256]{0:T(256)} %param.11) | copy-start | bytes 3076
  56.6 7.3 %copy-start.13 = (f32[64,512]{1,0:T(8,128)S(1)}, f32[64,512]{1,0:T(8,128)}, u32[]{:S(2)}) copy-start(f32[64,512]{1,0:T(8,128)} %param.17) | copy-start | bytes 393220
  60.1 18.4 %all-to-all-start = ((bf16[16,256,128]{2,1,0:T(8,128)(2,1)}), bf16[16,256,128]{2,1,0:T(8,128)(2,1)S(1)}, u32[]{:S(2)}, u32[]{:S(2)}) async-start(bf16[16,256,128]{2,1,0:T(8,128)(2,1)} %get-tuple-element.49), calls=%async_computation | async-start | bytes 2097152 | tf_op jit(solution)/shard_map/all_to_all | solution.py:45
  63.8 145.3 %all-gather.7.cloned.1.call-start = ((), (), s32[]{:S(2)}) async-start(), calls=%async_computation.9 | async-start | bytes 1114112 | tf_op jit(solution)/shard_map/all_gather | solution.py:61
  64.5 2.9 copy-start.2
  66.4 2.3 copy-start.10
  66.4 2.3 copy-start.12
  78.6 61.1 %copy-start.5 = (bf16[16,256,128]{2,1,0:T(8,128)(2,1)}, bf16[16,256,128]{2,1,0:T(8,128)(2,1)S(1)}, u32[]{:S(2)}) copy-start(bf16[16,256,128]{2,1,0:T(8,128)(2,1)S(1)} %all-to-all-done) | copy-start | bytes 3145732
  78.6 61.1 %all-to-all-start.1 = ((bf16[16,256,128]{2,1,0:T(8,128)(2,1)}), bf16[16,256,128]{2,1,0:T(8,128)(2,1)S(1)}, u32[]{:S(2)}, u32[]{:S(2)}) async-start(bf16[16,256,128]{2,1,0:T(8,128)(2,1)} %get-tuple-element.48), calls=%async_computation.1 | async-start | bytes 2097152 | tf_op jit(solution)/shard_map/all_to_all | solution.py:46
  82.2 171.0 %all-gather.11.cloned.1.call-start = ((), (), s32[]{:S(2)}) async-start(), calls=%async_computation.11 | async-start | bytes 4718592 | tf_op jit(solution)/shard_map/all_gather | solution.py:12
  139.7 7.0 %copy-start.7 = (bf16[16,256,128]{2,1,0:T(8,128)(2,1)}, bf16[16,256,128]{2,1,0:T(8,128)(2,1)S(1)}, u32[]{:S(2)}) copy-start(bf16[16,256,128]{2,1,0:T(8,128)(2,1)S(1)} %all-to-all-done.1) | copy-start | bytes 3145732
  209.1 24.5 %all-to-all-start.4 = ((bf16[8,128,512]{2,1,0:T(8,128)(2,1)}), bf16[8,128,512]{2,1,0:T(8,128)(2,1)}, u32[]{:S(2)}, u32[]{:S(2)}) async-start(bf16[8,128,512]{2,1,0:T(8,128)(2,1)} %bitcast.89), calls=%async_computation.4 | async-start | bytes 2097152 | tf_op jit(solution)/shard_map/all_to_all | solution.py:63
  214.4 22.9 %copy-start.14 = (s32[512,2]{0,1:T(2,128)S(1)}, s32[512,2]{0,1:T(2,128)}, u32[]{:S(2)}) copy-start(s32[512,2]{0,1:T(2,128)} %param.18) | copy-start | bytes 12292
  214.4 23.5 %copy-start.15 = (f32[512,2]{0,1:T(2,128)S(1)}, f32[512,2]{0,1:T(2,128)}, u32[]{:S(2)}) copy-start(f32[512,2]{0,1:T(2,128)} %param.19) | copy-start | bytes 12292
  233.6 19.7 %all-to-all-start.6 = ((bf16[128,8,512]{2,0,1:T(8,128)(2,1)}), bf16[128,8,512]{2,0,1:T(8,128)(2,1)S(1)}, u32[]{:S(2)}, u32[]{:S(2)}) async-start(bf16[128,8,512]{2,0,1:T(8,128)(2,1)} %bitcast.14), calls=%async_computation.6 | async-start | bytes 2097152 | tf_op jit(solution)/shard_map/all_to_all | solution.py:95
  253.3 3.3 %copy-start.3 = (bf16[2048,1024]{1,0:T(8,128)(2,1)S(1)}, bf16[2048,1024]{1,0:T(8,128)(2,1)}, u32[]{:S(2)}) copy-start(bf16[2048,1024]{1,0:T(8,128)(2,1)} %all-gather.11.cloned.1.call-done) | copy-start | bytes 12582916
  262.1 3.9 %copy-start.4 = (bf16[1024,512]{1,0:T(8,128)(2,1)S(1)}, bf16[1024,512]{1,0:T(8,128)(2,1)}, u32[]{:S(2)}) copy-start(bf16[1024,512]{1,0:T(8,128)(2,1)} %all-gather.7.cloned.1.call-done) | copy-start | bytes 3145732
  262.1 28.3 %all-to-all-start.7 = ((bf16[16,96,512]{2,1,0:T(8,128)(2,1)}), bf16[16,96,512]{2,1,0:T(8,128)(2,1)S(1)}, u32[]{:S(2)}, u32[]{:S(2)}) async-start(bf16[16,96,512]{2,1,0:T(8,128)(2,1)} %bitcast.24), calls=%async_computation.7 | async-start | bytes 3145728 | tf_op jit(solution)/shard_map/all_to_all | solution.py:100
  295.5 6.0 %copy-start.9 = (f32[512,512]{1,0:T(8,128)S(1)}, f32[512,512]{1,0:T(8,128)}, u32[]{:S(2)}) copy-start(f32[512,512]{1,0:T(8,128)} %fusion.10) | copy-start | bytes 3145732
  297.0 6.4 %copy-start.6 = (bf16[16,256,128]{2,1,0:T(8,128)(2,1)S(1)}, bf16[16,256,128]{2,1,0:T(8,128)(2,1)}, u32[]{:S(2)}) copy-start(bf16[16,256,128]{2,1,0:T(8,128)(2,1)} %copy-done.5) | copy-start | bytes 3145732
  297.1 7.4 %copy-start.8 = (bf16[16,256,128]{2,1,0:T(8,128)(2,1)S(1)}, bf16[16,256,128]{2,1,0:T(8,128)(2,1)}, u32[]{:S(2)}) copy-start(bf16[16,256,128]{2,1,0:T(8,128)(2,1)} %copy-done.7) | copy-start | bytes 3145732
Sparse Core Ops, SparseCore 0:
  10.7 52.8 all-gather.4
  65.3 67.9 all-gather.8
  135.9 44.8 all-gather.6
  183.0 52.5 all-gather.10
where the time goes:
time: 313 us; the launch traced here: 312 us
  waiting for transfers between devices  102 us (33%)
  blocking collectives  82.7 us (26%)
  matrix products  37 us (12%)
  other arithmetic  30.7 us (10%)
  local copies, waits for them, and re-layouts  25.9 us (8%)
  starting transfers between devices  19.4 us (6%)
  between operations  14.3 us (5%)
    all_gather x1, waiting for transfers between devices, on_device(): arrived = lax.all_gather(arriving, 'tp', axis=2, tiled=True)  51 us
    all_to_all x1, blocking collectives, on_device(): lax.all_to_all(outgoing, 'fs', split_axis=0, concat_axis=0, tiled=True)  33 us
    all_to_all x1, blocking collectives, on_device(): lax.all_to_all(down_train.astype(jnp.bfloat16), 'fs', split_axis=0, conca...  25.8 us
    all_to_all x1, blocking collectives, on_device(): lax.all_to_all(lax.all_to_all(down_train.astype(jnp.bfloat16), 'fs', spli...  24 us
    dot_general x16, matrix products, blockwise_down(): jnp.dot(hidden[:, block * step_width:(block + 1) * step_width], weight_do...  20.1 us
    all_to_all x1, waiting for transfers between devices, on_device(): lax.all_to_all(shared_down_rows, 'tp', split_axis=0, concat_axis=1, tiled...  17.9 us
    all_to_all x1, waiting for transfers between devices, on_device(): lax.all_to_all(returning, 'fs', split_axis=0, concat_axis=0, tiled=True)  15.1 us
    unnamed x44, local copies, waits for them, and re-layouts  11.2 us
  transfers between devices with their start and end apart: 9, of which 5 were waited for; matrix products, arithmetic and copies ran while one was open for 21% of the time, Pallas kernels for 0%

commit v1 on v0

--- a/solution.py
+++ b/solution.py
@@ -84,7 +84,8 @@
     outgoing = jnp.einsum("ts,td->sd", placing, own_columns, preferred_element_type=jnp.float32)
     outgoing = outgoing.astype(jnp.bfloat16).reshape(experts, capacity, columns)
     arriving = lax.all_to_all(outgoing, "fs", split_axis=0, concat_axis=0, tiled=True)
-    arrived = lax.all_gather(arriving, "tp", axis=2, tiled=True)
+    outgoing_2 = jnp.stack([arriving] * lax.axis_size("tp"))
+    arrived = jnp.concatenate(lax.all_to_all(outgoing_2, "tp", 0, 0), axis=2)
     arrived_rows = arrived.reshape(-1, model_width)
     gate_vals = jnp.dot(arrived_rows, expert_gate[0], preferred_element_type=jnp.float32)
     up_vals = jnp.dot(arrived_rows, expert_up[0], preferred_element_type=jnp.float32)

time: 313 us -> 416 us (1.33)
  waiting for transfers between devices: 102 us -> 183 us
  local copies, waits for them, and re-layouts: 25.9 us -> 51.4 us
  blocking collectives: 82.7 us -> 68.4 us
  starting transfers between devices: 19.4 us -> 28.5 us
    all_to_all x0 -> x1, waiting for transfers between devices: none -> 134 us  [on_device(): arrived = jnp.concatenate(lax.all_to_all(outgoing_2, 'tp', 0, 0), axis=2)]
    all_gather x1 -> x0, waiting for transfers between devices: 51 us -> none  [on_device(): arrived = lax.all_gather(arriving, 'tp', axis=2, tiled=True)]
    reshape x0 -> x1, local copies, waits for them, and re-layouts: none -> 12.1 us  [on_device(): arrived = jnp.concatenate(lax.all_to_all(outgoing_2, 'tp', 0, 0), axis=2)]
    all_to_all x1, waiting for transfers between devices: 0.01 us -> 10.5 us  [on_device(): lax.all_to_all(up_local, 'fs', split_axis=0, concat_axis=1, tiled=True)]
    all_to_all x1, waiting for transfers between devices: 8.59 us -> 0.01 us  [on_device(): lax.all_to_all(gate_local, 'fs', split_axis=0, concat_axis=1, tiled=True)]
    unnamed x44 -> x45, local copies, waits for them, and re-layouts: 11.2 us -> 18.6 us
    all_to_all x1, blocking collectives: 25.8 us -> 19.3 us  [on_device(): lax.all_to_all(down_train.astype(jnp.bfloat16), 'fs', split_axis=0, conca...]
    another operation x2 -> x3, local copies, waits for them, and re-layouts: 0.08 us -> 6.15 us  [the longest x1 6.07 us: on_device(): outgoing_2 = jnp.stack([arriving] * lax.axis_size('tp'))]
  transfers between devices with their start and end apart: 9 -> 9, of which waited for: 5 -> 5; matrix products, arithmetic and copies ran while one was open for 21% -> 18% of each run, Pallas kernels for 0% -> 0%
where the time goes in v1:
time: 416 us; the launch traced here: 415 us
  waiting for transfers between devices  183 us (44%)
  blocking collectives  68.4 us (16%)
  local copies, waits for them, and re-layouts  51.4 us (12%)
  matrix products  38.4 us (9%)
  other arithmetic  31.5 us (8%)
  starting transfers between devices  28.5 us (7%)
  between operations  14.3 us (3%)
    all_to_all x1, waiting for transfers between devices, on_device(): arrived = jnp.concatenate(lax.all_to_all(outgoing_2, 'tp', 0, 0), axis=2)  134 us
    all_to_all x1, blocking collectives, on_device(): lax.all_to_all(outgoing, 'fs', split_axis=0, concat_axis=0, tiled=True)  30.7 us
    dot_general x16, matrix products, blockwise_down(): jnp.dot(hidden[:, block * step_width:(block + 1) * step_width], weight_do...  20.5 us
    all_to_all x1, blocking collectives, on_device(): lax.all_to_all(down_train.astype(jnp.bfloat16), 'fs', split_axis=0, conca...  19.3 us
    unnamed x45, local copies, waits for them, and re-layouts  18.6 us
    all_to_all x1, blocking collectives, on_device(): lax.all_to_all(lax.all_to_all(down_train.astype(jnp.bfloat16), 'fs', spli...  18.4 us
    all_to_all x1, waiting for transfers between devices, on_device(): lax.all_to_all(returning, 'fs', split_axis=0, concat_axis=0, tiled=True)  15.2 us
    all_to_all x1, waiting for transfers between devices, on_device(): lax.all_to_all(shared_down_rows, 'tp', split_axis=0, concat_axis=1, tiled...  13.6 us
  transfers between devices with their start and end apart: 9, of which 5 were waited for; matrix products, arithmetic and copies ran while one was open for 18% of the time, Pallas kernels for 0%

profile of v1, /device:TPU:0, one launch (start us, length us, event | category | flops | bytes accessed | tf_op | source)
XLA Modules:
  0.0 415.2 jit_solution(6412491783498018611)
XLA Ops:
  8.4 4.5 %reduce-window.6 = s32[16,8,128]{2,1,0:T(8,128)S(1)} reduce-window(s32[16,8,128]{2,1,0:T(8,128)S(1)} %fusion.51, s32[]{:T(128)} %constant.18.clone.1), window={size=1x1x128 pad=0_0x0_0x127_0}, to_apply=%region_0.0 | reduce-window | flops 2080768 | bytes 131076 | tf_op jit(solution)/shard_map/reduce-window
  15.0 3.2 fusion
  18.4 3.4 fusion.1
  21.8 2.0 convolution_convert_fusion
  23.9 30.7 %all_to_all.104 = bf16[16,96,512]{2,1,0:T(8,128)(2,1)S(1)} all-to-all(bf16[16,96,512]{2,1,0:T(8,128)(2,1)S(1)} %bitcast.103), channel_id=1, replica_groups=mesh['fs'=16,'tp'=8] {'fs'}, dimensions={0} | all-to-all | bytes 3145728 | tf_op jit(solution)/shard_map/all_to_all | solution.py:86
  54.6 6.1 %stack.2 = bf16[8,16,96,512]{3,2,1,0:T(8,128)(2,1)} broadcast(bf16[16,96,512]{2,1,0:T(8,128)(2,1)S(1)} %all_to_all.104), dimensions={1,2,3} | broadcast | bytes 14155776 | tf_op jit(solution)/shard_map/stack | solution.py:87
  60.7 5.6 %all-to-all-start.6 = ((bf16[8,16,96,512]{3,2,1,0:T(8,128)(2,1)}), bf16[8,16,96,512]{3,2,1,0:T(8,128)(2,1)}, u32[]{:S(2)}, u32[]{:S(2)}) async-start(bf16[8,16,96,512]{3,2,1,0:T(8,128)(2,1)} %stack.2), calls=%async_computation.6 | async-start | bytes 25165824 | tf_op jit(solution)/shard_map/all_to_all | solution.py:88
  68.0 3.5 multiply_convert_fusion
  71.5 134.4 %all-to-all-done.6 = bf16[8,16,96,512]{3,2,1,0:T(8,128)(2,1)} async-done(((bf16[8,16,96,512]{3,2,1,0:T(8,128)(2,1)}), bf16[8,16,96,512]{3,2,1,0:T(8,128)(2,1)}, u32[]{:S(2)}, u32[]{:S(2)}) %all-to-all-start.6) | async-done | bytes 12582944 | tf_op jit(solution)/shard_map/all_to_all | solution.py:88
  205.9 3.8 all-to-all-start
  209.7 1.8 fusion.55
  215.1 12.1 %copy.83 = bf16[16,96,8,512]{3,2,1,0:T(8,128)(2,1)S(1)} copy(bf16[16,96,8,512]{3,1,0,2:T(8,128)(2,1)} %bitcast.11) | data formatting | bytes 25165824 | tf_op jit(solution)/shard_map/reshape | solution.py:88
  227.2 8.1 %copy.89 = bf16[192,8,8,512]{3,1,2,0:T(8,128)(2,1)} copy(bf16[192,8,8,512]{3,2,1,0:T(8,128)(2,1)S(1)} %bitcast.82) | data formatting | bytes 25165824
  235.3 7.0 %all-to-all-start.1 = ((bf16[16,256,128]{2,1,0:T(8,128)(2,1)}), bf16[16,256,128]{2,1,0:T(8,128)(2,1)S(1)}, u32[]{:S(2)}, u32[]{:S(2)}) async-start(bf16[16,256,128]{2,1,0:T(8,128)(2,1)} %get-tuple-element.48), calls=%async_computation.1 | async-start | bytes 2097152 | tf_op jit(solution)/shard_map/all_to_all | solution.py:46
  242.4 6.4 %fusion.56 = f32[1536,128]{1,0:T(8,128)S(1)} fusion(bf16[1536,4096]{1,0:T(8,128)(2,1)} %bitcast.83, bf16[4096,128]{1,0:T(8,128)(2,1)S(1)} %bitcast.97), kind=kOutput, calls=%fused_computation.106 | convolution fusion | flops 1610612736 | bytes 14417920 | tf_op jit(solution)/shard_map/dot_general | solution.py:90
  248.8 10.5 %all-to-all-done.1 = bf16[16,256,128]{2,1,0:T(8,128)(2,1)S(1)} async-done(((bf16[16,256,128]{2,1,0:T(8,128)(2,1)}), bf16[16,256,128]{2,1,0:T(8,128)(2,1)S(1)}, u32[]{:S(2)}, u32[]{:S(2)}) %all-to-all-start.1) | async-done | bytes 1048608 | tf_op jit(solution)/shard_map/all_to_all | solution.py:46
  259.3 7.0 %fusion.4 = bf16[1536,128]{1,0:T(8,128)(2,1)S(1)} fusion(bf16[1536,4096]{1,0:T(8,128)(2,1)} %bitcast.84, bf16[4096,128]{1,0:T(8,128)(2,1)S(1)} %bitcast.99, f32[1536,128]{1,0:T(8,128)S(1)} %fusion.56), kind=kOutput, calls=%fused_computation.19 | convolution fusion | flops 1611792384 | bytes 14811136 | tf_op jit(solution)/shard_map/dot_general | solution.py:91
  267.2 1.7 convert_element_type.153
  268.9 19.3 %all_to_all.105 = bf16[16,64,512]{2,1,0:T(8,128)(2,1)S(1)} all-to-all(bf16[16,64,512]{2,1,0:T(8,128)(2,1)S(1)} %convert_element_type.153), channel_id=1, replica_groups=mesh['fs'=16,'tp'=8] {'fs'}, dimensions={0} | all-to-all | bytes 2097152 | tf_op jit(solution)/shard_map/all_to_all | solution.py:49
  290.3 7.0 %reduce.1 = bf16[1024,512]{1,0:T(8,128)(2,1)S(1)} reduce(bf16[1024,1,512]{2,1,0:T(2,128)(2,1)S(1)} %bitcast.86, bf16[]{:T(256)} %broadcast.93), dimensions={1}, to_apply=%bitcast.80.reduce_sub_computation | reduce | bytes 2097154
  298.2 18.4 %all_to_all.106 = bf16[8,2,32768]{2,1,0:T(2,128)(2,1)S(1)} all-to-all(bf16[8,2,32768]{2,1,0:T(2,128)(2,1)S(1)} %reshape.156), channel_id=1, replica_groups=mesh['fs'=16,'tp'=8] {'tp'}, dimensions={0} | all-to-all | bytes 2097152 | tf_op jit(solution)/shard_map/all_to_all | solution.py:48
  316.6 4.2 %all-to-all-start.4 = ((bf16[8,128,512]{2,1,0:T(8,128)(2,1)}), bf16[8,128,512]{2,1,0:T(8,128)(2,1)}, u32[]{:S(2)}, u32[]{:S(2)}) async-start(bf16[8,128,512]{2,1,0:T(8,128)(2,1)} %bitcast.95), calls=%async_computation.4 | async-start | bytes 2097152 | tf_op jit(solution)/shard_map/all_to_all | solution.py:63
  323.2 13.6 %all-to-all-done.4 = bf16[8,128,512]{2,1,0:T(8,128)(2,1)} async-done(((bf16[8,128,512]{2,1,0:T(8,128)(2,1)}), bf16[8,128,512]{2,1,0:T(8,128)(2,1)}, u32[]{:S(2)}, u32[]{:S(2)}) %all-to-all-start.4) | async-done | bytes 1048608 | tf_op jit(solution)/shard_map/all_to_all | solution.py:63
  336.8 3.8 all-to-all-start.7
  347.2 9.0 %all-to-all-done.7 = bf16[128,8,512]{2,0,1:T(8,128)(2,1)S(1)} async-done(((bf16[128,8,512]{2,0,1:T(8,128)(2,1)}), bf16[128,8,512]{2,0,1:T(8,128)(2,1)S(1)}, u32[]{:S(2)}, u32[]{:S(2)}) %all-to-all-start.7) | async-done | bytes 1048608 | tf_op jit(solution)/shard_map/all_to_all | solution.py:96
  362.2 2.8 add_convert_fusion
  365.1 3.8 all-to-all-start.8
  376.1 2.2 fusion.10
  378.2 15.2 %all-to-all-done.8 = bf16[16,96,512]{2,1,0:T(8,128)(2,1)S(1)} async-done(((bf16[16,96,512]{2,1,0:T(8,128)(2,1)}), bf16[16,96,512]{2,1,0:T(8,128)(2,1)S(1)}, u32[]{:S(2)}, u32[]{:S(2)}) %all-to-all-start.8) | async-done | bytes 1572896 | tf_op jit(solution)/shard_map/all_to_all | solution.py:101
  393.4 5.1 %gather_fusion = bf16[1024,512]{1,0:T(8,128)(2,1)} fusion(bf16[1536,512]{1,0:T(8,128)(2,1)S(1)} %bitcast.81, s32[1024]{0:T(1024)S(1)} %broadcast_clamp_fusion), kind=kCustom, calls=%fused_computation | custom fusion | bytes 2101248 | tf_op jit(solution)/shard_map/jit(_take)/gather | solution.py:104
  400.0 4.4 %multiply_reduce_fusion = f32[512,512]{1,0:T(8,128)S(1)} fusion(bf16[512,2,512]{2,1,0:T(2,128)(2,1)S(1)} %gather.7, pred[512,2]{1,0:T(8,128)(4,1)S(1)} %copy.82, f32[512,2]{1,0:T(8,128)S(1)} %copy.76), kind=kLoop, calls=%fused_computation.20 | loop fusion | flops 1835008 | bytes 2102272 | tf_op jit(solution)/shard_map/reduce_sum | solution.py:105
  404.4 2.4 fusion.8
  (98 shorter events, 37.8 us)
Async XLA Ops:
  15.0 3.5 copy-start
  60.7 5.7 %copy-start.11 = (f32[256,128]{1,0:T(8,128)S(1)}, f32[256,128]{1,0:T(8,128)}, u32[]{:S(2)}) copy-start(f32[256,128]{1,0:T(8,128)} %param.15) | copy-start | bytes 393220
  60.7 5.7 %copy-start.12 = (f32[256,128]{1,0:T(8,128)S(1)}, f32[256,128]{1,0:T(8,128)}, u32[]{:S(2)}) copy-start(f32[256,128]{1,0:T(8,128)} %param.16) | copy-start | bytes 393220
  60.7 5.7 %copy-start.16 = (f32[256]{0:T(256)S(1)}, f32[256]{0:T(256)}, u32[]{:S(2)}) copy-start(f32[256]{0:T(256)} %param.11) | copy-start | bytes 3076
  60.7 6.6 %copy-start.13 = (f32[64,512]{1,0:T(8,128)S(1)}, f32[64,512]{1,0:T(8,128)}, u32[]{:S(2)}) copy-start(f32[64,512]{1,0:T(8,128)} %param.17) | copy-start | bytes 393220
  60.7 7.3 %copy-start.9 = (f32[16,256,128]{2,1,0:T(8,128)S(1)}, f32[16,256,128]{2,1,0:T(8,128)}, u32[]{:S(2)}) copy-start(f32[16,256,128]{2,1,0:T(8,128)} %param.13) | copy-start | bytes 6291460
  60.7 145.2 %all-to-all-start.6 = ((bf16[8,16,96,512]{3,2,1,0:T(8,128)(2,1)}), bf16[8,16,96,512]{3,2,1,0:T(8,128)(2,1)}, u32[]{:S(2)}, u32[]{:S(2)}) async-start(bf16[8,16,96,512]{3,2,1,0:T(8,128)(2,1)} %stack.2), calls=%async_computation.6 | async-start | bytes 25165824 | tf_op jit(solution)/shard_map/all_to_all | solution.py:88
  66.3 143.4 %all-gather.4.cloned.1.call-start = ((), (), s32[]{:S(2)}) async-start(), calls=%async_computation.9 | async-start | bytes 2228224 | tf_op jit(solution)/shard_map/all_gather | solution.py:12
  67.2 249.4 %all-gather.6.cloned.1.call-start = ((), (), s32[]{:S(2)}) async-start(), calls=%async_computation.10 | async-start | bytes 1114112 | tf_op jit(solution)/shard_map/all_gather | solution.py:61
  205.9 29.5 %all-to-all-start = ((bf16[16,256,128]{2,1,0:T(8,128)(2,1)}), bf16[16,256,128]{2,1,0:T(8,128)(2,1)S(1)}, u32[]{:S(2)}, u32[]{:S(2)}) async-start(bf16[16,256,128]{2,1,0:T(8,128)(2,1)} %get-tuple-element.49), calls=%async_computation | async-start | bytes 2097152 | tf_op jit(solution)/shard_map/all_to_all | solution.py:45
  209.7 2.9 copy-start.1
  211.6 3.6 copy-start.8
  211.6 3.6 copy-start.10
  235.3 13.5 %copy-start.4 = (bf16[16,256,128]{2,1,0:T(8,128)(2,1)}, bf16[16,256,128]{2,1,0:T(8,128)(2,1)S(1)}, u32[]{:S(2)}) copy-start(bf16[16,256,128]{2,1,0:T(8,128)(2,1)S(1)} %all-to-all-done) | copy-start | bytes 3145732
  235.3 23.9 %all-to-all-start.1 = ((bf16[16,256,128]{2,1,0:T(8,128)(2,1)}), bf16[16,256,128]{2,1,0:T(8,128)(2,1)S(1)}, u32[]{:S(2)}, u32[]{:S(2)}) async-start(bf16[16,256,128]{2,1,0:T(8,128)(2,1)} %get-tuple-element.48), calls=%async_computation.1 | async-start | bytes 2097152 | tf_op jit(solution)/shard_map/all_to_all | solution.py:46
  242.3 113.9 %all-gather.8.cloned.1.call-start = ((), (), s32[]{:S(2)}) async-start(), calls=%async_computation.11 | async-start | bytes 4718592 | tf_op jit(solution)/shard_map/all_gather | solution.py:12
  259.3 7.0 %copy-start.6 = (bf16[16,256,128]{2,1,0:T(8,128)(2,1)}, bf16[16,256,128]{2,1,0:T(8,128)(2,1)S(1)}, u32[]{:S(2)}) copy-start(bf16[16,256,128]{2,1,0:T(8,128)(2,1)S(1)} %all-to-all-done.1) | copy-start | bytes 3145732
  316.6 20.2 %all-to-all-start.4 = ((bf16[8,128,512]{2,1,0:T(8,128)(2,1)}), bf16[8,128,512]{2,1,0:T(8,128)(2,1)}, u32[]{:S(2)}, u32[]{:S(2)}) async-start(bf16[8,128,512]{2,1,0:T(8,128)(2,1)} %bitcast.95), calls=%async_computation.4 | async-start | bytes 2097152 | tf_op jit(solution)/shard_map/all_to_all | solution.py:63
  321.9 18.7 %copy-start.14 = (s32[512,2]{0,1:T(2,128)S(1)}, s32[512,2]{0,1:T(2,128)}, u32[]{:S(2)}) copy-start(s32[512,2]{0,1:T(2,128)} %param.18) | copy-start | bytes 12292
  321.9 19.3 %copy-start.15 = (f32[512,2]{0,1:T(2,128)S(1)}, f32[512,2]{0,1:T(2,128)}, u32[]{:S(2)}) copy-start(f32[512,2]{0,1:T(2,128)} %param.19) | copy-start | bytes 12292
  336.8 19.4 %all-to-all-start.7 = ((bf16[128,8,512]{2,0,1:T(8,128)(2,1)}), bf16[128,8,512]{2,0,1:T(8,128)(2,1)S(1)}, u32[]{:S(2)}, u32[]{:S(2)}) async-start(bf16[128,8,512]{2,0,1:T(8,128)(2,1)} %bitcast.14), calls=%async_computation.7 | async-start | bytes 2097152 | tf_op jit(solution)/shard_map/all_to_all | solution.py:96
  356.2 3.3 copy-start.2
  365.1 3.9 copy-start.3
  365.1 28.3 %all-to-all-start.8 = ((bf16[16,96,512]{2,1,0:T(8,128)(2,1)}), bf16[16,96,512]{2,1,0:T(8,128)(2,1)S(1)}, u32[]{:S(2)}, u32[]{:S(2)}) async-start(bf16[16,96,512]{2,1,0:T(8,128)(2,1)} %bitcast.24), calls=%async_computation.8 | async-start | bytes 3145728 | tf_op jit(solution)/shard_map/all_to_all | solution.py:101
  399.9 6.8 %copy-start.5 = (bf16[16,256,128]{2,1,0:T(8,128)(2,1)S(1)}, bf16[16,256,128]{2,1,0:T(8,128)(2,1)}, u32[]{:S(2)}) copy-start(bf16[16,256,128]{2,1,0:T(8,128)(2,1)} %copy-done.4) | copy-start | bytes 3145732
  400.0 7.8 %copy-start.7 = (bf16[16,256,128]{2,1,0:T(8,128)(2,1)S(1)}, bf16[16,256,128]{2,1,0:T(8,128)(2,1)}, u32[]{:S(2)}) copy-start(bf16[16,256,128]{2,1,0:T(8,128)(2,1)} %copy-done.6) | copy-start | bytes 3145732
Sparse Core Ops, SparseCore 0:
  69.8 42.9 all-gather.3
  115.5 41.8 all-gather.5
  267.3 30.5 all-gather.7
